TPU v7x, 32 devices: a whole 2x2x4 slice. The times are simulated.
32 devices in a mesh: grp: 2 (over y), ep: 4 (over z), tp: 4 (over x, core).
Axes of the slice: x: 2, y: 2, z: 4, core: 2. Of those that a mesh axis runs over, the one named last changes fastest.
Arguments:
- queries: bfloat16 [1024, 1024], P(('grp', 'ep'), 'tp'), parts along dimension 0, may hold values from -6 to 6
- keys: bfloat16 [1024, 1024], P(('grp', 'ep'), 'tp'), parts along dimension 0, may hold values from -6 to 6
- values: bfloat16 [1024, 1024], P(('grp', 'ep'), 'tp'), parts along dimension 0, may hold values from -6 to 6
- lambdas: float32 [8], P('tp'), may hold values from 0.3 to 0.8
- head_gain: float32 [128], replicated, may hold values from 0.1 to 1.9
- tokens: bfloat16 [2048, 1536], P(('grp', 'ep')), parts along dimension 0, may hold values from -6 to 6
- route_ids: int32 [2048, 2], P(('grp', 'ep')), parts along dimension 0, may hold values from 0 to 3, all different within a row; in each aligned block of 256 rows (0 to 255, 256 to 511, ...) at most 256 rows name the same one
- route_weights: float32 [2048, 2], P(('grp', 'ep')), parts along dimension 0, may hold values from 0.2 to 1
- moe_gain: float32 [1536], replicated, may hold values from 0.1 to 1.9
- w_gate: bfloat16 [4, 1536, 3072], P('ep', None, 'tp'), may hold values from -0.15625 to 0.15625
- w_up: bfloat16 [4, 1536, 3072], P('ep', None, 'tp'), may hold values from -0.15625 to 0.15625
- w_down: bfloat16 [4, 3072, 1536], P('ep', 'tp'), may hold values from -0.109375 to 0.109375
Outputs:
- heads_out: bfloat16 [1024, 1024], P(('grp', 'ep'), 'tp'), parts along dimension 0
- expert_out: bfloat16 [2048, 1536], P(('grp', 'ep'), 'tp'), parts along dimension 0
There are 2 independent parts, one for each index of `grp`. A program takes and returns all parts, laid end to end along the dimension named above; an argument that names none is the same for every part. Nothing has to cross between parts.
Inputs may be any that keep to these rules, and one draw needn't show every extreme that they name: `route_ids`: each row names 2 different experts. In the 256 rows of one device no expert is named more than 256 times, and in every draw some device names some expert exactly 256 times.
All inputs are finite; a program needn't handle non-finite values.
Results may differ from a plain program's by a relative error of at most 0.015.
Values may be sent and summed in bfloat16 or wider, within the bound.
A program may use at most 64 MiB of HBM per device.

v0:
```python
import jax
import jax.numpy as jnp
from jax import lax
from jax.sharding import PartitionSpec as P


def attend(queries, keys, values, lambdas, head_gain):
    row_count = queries.shape[0]
    head_count = lambdas.shape[0]
    head_dim = queries.shape[1] // (2 * head_count)
    value_dim = values.shape[1] // head_count
    query_parts = queries.reshape(row_count, head_count, 2, head_dim)
    score_scale = head_dim ** (-0.5)
    running = jnp.full((head_count, 2, row_count), -1e30, jnp.float32)
    key_piece = lax.all_gather(keys, "ep", axis=0, tiled=True)
    value_piece = lax.all_gather(values, "ep", axis=0, tiled=True)
    count = key_piece.shape[0]
    key_parts = key_piece.reshape(count, head_count, 2, head_dim)
    value_parts = value_piece.reshape(count, head_count, value_dim)
    scores = (
        jnp.einsum("qhcd,khcd->hcqk", query_parts, key_parts, preferred_element_type=jnp.float32)
        * score_scale
    )
    newest = jnp.maximum(running, jnp.max(scores, axis=-1))
    weights_now = jnp.exp(scores - newest[..., None])
    totals = jnp.sum(weights_now, axis=-1)
    sums = jnp.einsum(
        "hcqk,khe->hcqe",
        weights_now.astype(jnp.bfloat16),
        value_parts,
        preferred_element_type=jnp.float32,
    )
    running, totals, sums = (newest, totals, sums)
    means = sums / totals[..., None]
    mixed = means[:, 0] - lambdas[:, None, None] * means[:, 1]
    scaled = mixed * lax.rsqrt(jnp.mean(mixed * mixed, axis=-1, keepdims=True) + 1e-06) * head_gain
    return (
        jnp.transpose(scaled, (1, 0, 2))
        .reshape(row_count, head_count * value_dim)
        .astype(jnp.bfloat16)
    )


def experts(tokens, route_ids, route_weights, moe_gain, w_gate, w_up, w_down):
    row_count, width = tokens.shape
    top_count = route_ids.shape[1]
    ep_size = lax.axis_size("ep")
    tp_size = lax.axis_size("tp")
    expert_count = w_gate.shape[0] * ep_size
    capacity = 2 * row_count * top_count // expert_count
    token_float = tokens.astype(jnp.float32)
    normed = (
        token_float
        * lax.rsqrt(jnp.mean(token_float * token_float, axis=1, keepdims=True) + 1e-06)
        * moe_gain
    ).astype(jnp.bfloat16)
    flat_ids = route_ids.reshape(-1)
    onehot = (flat_ids[:, None] == jnp.arange(expert_count, dtype=jnp.int32)[None, :]).astype(
        jnp.int32
    )
    earlier = jnp.cumsum(onehot, axis=0) - onehot
    position = jnp.sum(earlier * onehot, axis=1)
    slot_index = flat_ids * capacity + position
    owners = (
        jnp.full((expert_count * capacity,), row_count, jnp.int32)
        .at[slot_index]
        .set(jnp.arange(row_count * top_count, dtype=jnp.int32) // top_count)
    )
    padded = jnp.concatenate([normed, jnp.zeros((1, width), jnp.bfloat16)], axis=0)
    outgoing = padded[owners].reshape(expert_count, capacity, width)
    gate_mat = w_gate[0]
    up_mat = w_up[0]
    down_mat = w_down[0]
    slice_width = width // tp_size
    own_columns = lax.dynamic_slice_in_dim(
        outgoing, lax.axis_index("tp") * slice_width, slice_width, 2
    )
    arrived = lax.all_to_all(own_columns, "ep", split_axis=0, concat_axis=0, tiled=True)
    piece = lax.all_gather(arrived, "tp", axis=2, tiled=True)
    gate = jnp.einsum("scd,df->scf", piece, gate_mat, preferred_element_type=jnp.float32)
    upward = jnp.einsum("scd,df->scf", piece, up_mat, preferred_element_type=jnp.float32)
    hidden = (jax.nn.silu(gate) * upward).astype(jnp.bfloat16)
    flat_hidden = hidden.reshape(-1, hidden.shape[2])
    summed = lax.psum_scatter(
        jnp.einsum("fd,sf->ds", down_mat, flat_hidden, preferred_element_type=jnp.float32).astype(
            jnp.bfloat16
        ),
        "tp",
        scatter_dimension=0,
        tiled=True,
    )
    back = lax.all_to_all(summed, "ep", split_axis=1, concat_axis=1, tiled=True)
    picked = (
        jnp.take(back, slot_index, axis=1).astype(jnp.float32).reshape(-1, row_count, top_count)
    )
    combined = jnp.einsum("drk,rk->rd", picked, route_weights)
    return combined.astype(jnp.bfloat16)


def on_device(
    queries,
    keys,
    values,
    lambdas,
    head_gain,
    tokens,
    route_ids,
    route_weights,
    moe_gain,
    w_gate,
    w_up,
    w_down,
):
    heads_out = attend(queries, keys, values, lambdas, head_gain)
    expert_out = experts(tokens, route_ids, route_weights, moe_gain, w_gate, w_up, w_down)
    return (heads_out, expert_out)


def solution(mesh):
    in_specs = (
        P(("grp", "ep"), "tp"),
        P(("grp", "ep"), "tp"),
        P(("grp", "ep"), "tp"),
        P("tp"),
        P(),
        P(("grp", "ep"), None),
        P(("grp", "ep"), None),
        P(("grp", "ep"), None),
        P(),
        P("ep", None, "tp"),
        P("ep", None, "tp"),
        P("ep", "tp", None),
    )
    out_specs = (P(("grp", "ep"), "tp"), P(("grp", "ep"), "tp"))
    return jax.shard_map(
        on_device, mesh=mesh, in_specs=in_specs, out_specs=out_specs, check_vma=False
    )
```

profile of v0, /device:TPU:0, one launch (start us, length us, event | category | flops | bytes accessed | tf_op | source)
XLA Modules:
  0.0 183.2 jit_solution(15858981580019613275)
XLA Ops:
  7.2 0.0 copy-start
  7.2 0.0 all-gather.2.cloned.1.call-start
  7.2 1.0 copy.40
  8.2 0.1 eq.26
  8.3 0.1 reshape.111
  8.5 0.7 broadcast_multiply_fusion
  9.2 1.2 reduce-window.6
  10.4 0.2 slice_reduce_fusion
  10.6 0.2 reduce-window.9
  10.8 0.1 add_bitcast_fusion
  10.9 0.1 copy.44
  11.0 0.1 mul.101
  11.2 2.4 %scatter_custom_fusion = s32[1024]{0:T(1024)S(1)} fusion(s32[512]{0:T(512)S(1)} %bitcast.95, s32[512]{0:T(512)S(1)} %add_select_fusion, s32[]{:T(128)} %constant.33.clone.1), kind=kCustom, calls=%fused_computation.53 | custom fusion | bytes 4100 | tf_op jit(solution)/shard_map/scatter | solution.py:67
  13.7 1.4 fusion.8
  15.1 1.4 fusion.10
  16.4 0.1 concatenate.3
  16.5 5.6 %gather_fusion = bf16[1024,1536]{1,0:T(8,128)(2,1)} fusion(bf16[257,1536]{1,0:T(8,128)(2,1)S(1)} %concatenate.3, s32[1024]{0:T(1024)S(1)} %fusion.23), kind=kCustom, calls=%fused_computation | custom fusion | bytes 6295552 | tf_op jit(solution)/shard_map/gather | solution.py:70
  22.1 1.2 constant_dynamic-slice_fusion
  23.3 26.4 %all_to_all.17 = bf16[4,256,384]{2,1,0:T(8,128)(2,1)} all-to-all(bf16[4,256,384]{2,1,0:T(8,128)(2,1)S(1)} %constant_dynamic-slice_fusion), channel_id=1, replica_groups=mesh['grp'=2,'ep'=4,'tp'=4] {'ep'}, dimensions={0} | all-to-all | bytes 1572864 | tf_op jit(solution)/shard_map/all_to_all | solution.py:78
  49.7 0.0 all-gather.2.cloned.1.call-update
  49.7 0.0 reduce-scatter.4.cloned.1.call-start
  49.8 27.7 %all-gather.2.cloned.1.call-done = bf16[4,256,1536]{2,1,0:T(8,128)(2,1)} async-done(((bf16[4,256,384]{2,1,0:T(8,128)(2,1)}), bf16[4,256,1536]{2,1,0:T(8,128)(2,1)}) %all-gather.2.cloned.1.call-update) | async-done | bytes 3145744 | tf_op jit(solution)/shard_map/all_gather | solution.py:79
  77.4 0.0 copy-start.9
  77.5 5.4 %fusion.2 = f32[4,256,768]{2,1,0:T(8,128)S(1)} fusion(bf16[4,256,1536]{2,1,0:T(8,128)(2,1)} %all-gather.2.cloned.1.call-done, bf16[1,1536,768]{2,1,0:T(8,128)(2,1)} %param.22), kind=kOutput, calls=%fused_computation.7 | convolution fusion | flops 2415919104 | bytes 8650752 | tf_op jit(solution)/shard_map/scd,df->scf/dot_general | solution.py:81
  82.8 0.0 copy-done.8
  82.8 0.0 copy-done.9
  82.8 2.9 %multiply_convert_fusion = bf16[4,256,768]{2,1,0:T(8,128)(2,1)S(1)} fusion(f32[4,256,768]{2,1,0:T(8,128)S(1)} %fusion.2, bf16[4,256,1536]{2,1,0:T(8,128)(2,1)S(1)} %copy-done.8, bf16[1,1536,768]{2,1,0:T(8,128)(2,1)S(1)} %copy-done.9), kind=kOutput, calls=%fused_computation.5 | convolution fusion | flops 2420637696 | bytes 10223616 | tf_op jit(solution)/shard_map/scd,df->scf/dot_general | solution.py:80
  85.7 0.0 copy-done
  85.8 4.0 %fusion = bf16[1536,1024]{0,1:T(8,128)(2,1)} fusion(bf16[1024,768]{1,0:T(8,128)(2,1)S(1)} %bitcast.99, bf16[1,768,1536]{2,1,0:T(8,128)(2,1)S(1)} %copy-done), kind=kOutput, calls=%fused_computation.4 | convolution fusion | flops 2417491968 | bytes 7077888 | tf_op jit(solution)/shard_map/fd,sf->ds/dot_general | solution.py:85
  89.8 4.6 %copy.49 = bf16[1536,1024]{1,0:T(8,128)(2,1)} copy(bf16[1536,1024]{0,1:T(8,128)(2,1)} %fusion) | data formatting | bytes 6291456
  94.4 0.0 copy-start.4
  94.4 0.0 copy-start.5
  94.4 0.0 reduce-scatter.4.cloned.1.call-update
  94.5 0.0 copy-start.2
  94.5 0.1 reduce_sum.43
  94.6 0.1 copy.42
  94.7 0.4 copy-done.4
  95.1 0.8 copy.43
  95.9 0.0 copy-done.5
  95.9 0.8 copy.47
  96.7 0.0 copy-done.1
  96.7 13.9 %all_gather.9 = bf16[512,256]{1,0:T(8,128)(2,1)S(1)} all-gather(bf16[128,256]{1,0:T(8,128)(2,1)S(1)} %copy-done.1), channel_id=1, replica_groups=mesh['grp'=2,'ep'=4,'tp'=4] {'ep'}, dimensions={0}, use_global_device_ids=true | all-gather | bytes 327680 | tf_op jit(solution)/shard_map/all_gather | solution.py:15
  110.6 0.1 copy.37
  110.8 0.0 copy-done.3
  110.8 0.1 copy.36
  110.9 1.3 fusion.30
  112.2 20.3 %reduce-scatter.4.cloned.1.call-done = bf16[384,1024]{1,0:T(8,128)(2,1)} async-done(((bf16[1536,1024]{1,0:T(8,128)(2,1)}), bf16[384,1024]{1,0:T(8,128)(2,1)}) %reduce-scatter.4.cloned.1.call-update) | async-done | bytes 786448
  132.5 2.3 %copy.50 = bf16[384,1024]{0,1:T(8,128)(2,1)} copy(bf16[384,1024]{1,0:T(8,128)(2,1)} %reduce-scatter.4.cloned.1.call-done) | data formatting | bytes 1572864
  134.8 4.7 %all-to-all-start.1 = ((bf16[384,4,256]{0,2,1:T(8,128)(2,1)}), bf16[384,4,256]{0,2,1:T(8,128)(2,1)S(1)}, u32[]{:S(2)}, u32[]{:S(2)}) async-start(bf16[384,4,256]{0,2,1:T(8,128)(2,1)} %bitcast.87), calls=%async_computation.1 | async-start | bytes 1572864 | tf_op jit(solution)/shard_map/all_to_all | solution.py:92
  139.5 0.0 copy-done.2
  139.5 27.2 %all_gather.10 = bf16[512,256]{1,0:T(8,128)(2,1)S(1)} all-gather(bf16[128,256]{1,0:T(8,128)(2,1)S(1)} %copy-done.2), channel_id=1, replica_groups=mesh['grp'=2,'ep'=4,'tp'=4] {'ep'}, dimensions={0}, use_global_device_ids=true | all-gather | bytes 327680 | tf_op jit(solution)/shard_map/all_gather | solution.py:16
  166.7 0.9 copy.38
  167.6 1.5 fusion.11
  169.1 1.7 convolution_divide_fusion
  170.9 0.0 copy-done.6
  170.9 0.1 multiply_reduce_fusion
  171.0 0.0 copy-done.7
  171.0 0.1 multiply_convert_fusion.1
  171.1 0.7 copy.45
  171.8 0.0 all-to-all-done.1
  171.8 1.9 %gather_fusion.1 = bf16[512,384]{1,0:T(8,128)(2,1)S(1)} fusion(bf16[384,1024]{0,1:T(8,128)(2,1)S(1)} %bitcast.85, s32[1024]{0:T(1024)S(1)} %pad_clamp_fusion), kind=kCustom, calls=%fused_computation.1 | custom fusion | bytes 788480 | tf_op jit(solution)/shard_map/jit(_take)/gather | solution.py:94
  173.8 0.1 gather.11
  173.9 1.7 fusion.15
  175.7 0.7 copy.55
  (15 shorter events, 0.1 us)
Async XLA Ops:
  7.2 78.6 %copy-start = (bf16[1,768,1536]{2,1,0:T(8,128)(2,1)S(1)}, bf16[1,768,1536]{2,1,0:T(8,128)(2,1)}, u32[]{:S(2)}) copy-start(bf16[1,768,1536]{2,1,0:T(8,128)(2,1)} %param.23) | copy-start | bytes 7077892
  7.2 70.3 %all-gather.2.cloned.1.call-start = ((), (), s32[]{:S(2)}) async-start(), calls=%async_computation.3 | async-start | bytes 3932160 | tf_op jit(solution)/shard_map/all_gather | solution.py:79
  49.7 82.8 %reduce-scatter.4.cloned.1.call-start = ((), (), s32[]{:S(2)}) async-start(), calls=%async_computation.4 | async-start | bytes 3932160
  77.4 5.4 %copy-start.8 = (bf16[4,256,1536]{2,1,0:T(8,128)(2,1)S(1)}, bf16[4,256,1536]{2,1,0:T(8,128)(2,1)}, u32[]{:S(2)}) copy-start(bf16[4,256,1536]{2,1,0:T(8,128)(2,1)} %all-gather.2.cloned.1.call-done) | copy-start | bytes 9437188
  77.4 5.4 %copy-start.9 = (bf16[1,1536,768]{2,1,0:T(8,128)(2,1)S(1)}, bf16[1,1536,768]{2,1,0:T(8,128)(2,1)}, u32[]{:S(2)}) copy-start(bf16[1,1536,768]{2,1,0:T(8,128)(2,1)} %param.21) | copy-start | bytes 7077892
  94.4 0.7 copy-start.4
  94.4 1.4 copy-start.5
  94.4 2.3 %copy-start.1 = (bf16[128,256]{1,0:T(8,128)(2,1)S(1)}, bf16[128,256]{1,0:T(8,128)(2,1)}, u32[]{:S(2)}) copy-start(bf16[128,256]{1,0:T(8,128)(2,1)} %param.13) | copy-start | bytes 196612
  94.4 16.4 %copy-start.3 = (bf16[128,256]{1,0:T(8,128)(2,1)S(1)}, bf16[128,256]{1,0:T(8,128)(2,1)}, u32[]{:S(2)}) copy-start(bf16[128,256]{1,0:T(8,128)(2,1)} %param.12) | copy-start | bytes 196612
  94.5 45.1 %copy-start.2 = (bf16[128,256]{1,0:T(8,128)(2,1)S(1)}, bf16[128,256]{1,0:T(8,128)(2,1)}, u32[]{:S(2)}) copy-start(bf16[128,256]{1,0:T(8,128)(2,1)} %param.14) | copy-start | bytes 196612
  112.2 58.6 %copy-start.6 = (f32[2]{0:T(128)S(1)}, f32[2]{0:T(128)}, u32[]{:S(2)}) copy-start(f32[2]{0:T(128)} %param.15) | copy-start | bytes 28
  134.8 36.2 %copy-start.7 = (f32[128]{0:T(128)S(1)}, f32[128]{0:T(128)}, u32[]{:S(2)}) copy-start(f32[128]{0:T(128)} %param.16) | copy-start | bytes 1540
  134.8 37.1 %all-to-all-start.1 = ((bf16[384,4,256]{0,2,1:T(8,128)(2,1)}), bf16[384,4,256]{0,2,1:T(8,128)(2,1)S(1)}, u32[]{:S(2)}, u32[]{:S(2)}) async-start(bf16[384,4,256]{0,2,1:T(8,128)(2,1)} %bitcast.87), calls=%async_computation.1 | async-start | bytes 1572864 | tf_op jit(solution)/shard_map/all_to_all | solution.py:92
Sparse Core Ops, SparseCore 0:
  49.8 27.5 all-gather.1
  94.6 37.8 reduce-scatter.3
where the time goes:
time: 184 us; the launch traced here: 183 us
  blocking collectives  67.5 us (37%)
  waiting for transfers between devices  48 us (26%)
  local copies, waits for them, and re-layouts  24.9 us (14%)
  matrix products  17 us (9%)
  between operations  14.3 us (8%)
  other arithmetic  6.72 us (4%)
  starting transfers between devices  4.81 us (3%)
    all_gather x1, waiting for transfers between devices, experts(): piece = lax.all_gather(arrived, 'tp', axis=2, tiled=True)  27.7 us
    all_gather x1, blocking collectives, attend(): value_piece = lax.all_gather(values, 'ep', axis=0, tiled=True)  27.2 us
    all_to_all x1, blocking collectives, experts(): lax.all_to_all(own_columns, 'ep', split_axis=0, concat_axis=0, tiled=True)  26.4 us
    unnamed x3, waiting for transfers between devices  20.3 us
    all_gather x1, blocking collectives, attend(): key_piece = lax.all_gather(keys, 'ep', axis=0, tiled=True)  13.9 us
    unnamed x26, local copies, waits for them, and re-layouts  10 us
    gather x1, local copies, waits for them, and re-layouts, experts(): outgoing = padded[owners].reshape(expert_count, capacity, width)  5.61 us
    dot_general x1, matrix products, experts(): jnp.einsum('scd,df->scf', piece, up_mat, preferred_element_type=jnp.float32)  5.36 us
  transfers between devices with their start and end apart: 3, of which 2 were waited for; matrix products, arithmetic and copies ran while one was open for 5% of the time, Pallas kernels for 0%

commit v1 on v0

--- a/solution.py
+++ b/solution.py
@@ -2,6 +2,17 @@
 import jax.numpy as jnp
 from jax import lax
 from jax.sharding import PartitionSpec as P
+
+
+def pass_along(x, name, dim):
+    n_dev = lax.axis_size(name)
+    right = [(i, (i + 1) % n_dev) for i in range(n_dev)]
+    parts = [x]
+    for far in range(1, n_dev):
+        parts = [lax.ppermute(parts[0], name, right), *parts]
+    out = jnp.concatenate(parts, axis=dim)
+    shift = (lax.axis_index(name) + 1) * parts[-1].shape[dim]
+    return jnp.roll(out, shift, axis=dim)
 
 
 def attend(queries, keys, values, lambdas, head_gain):
@@ -13,7 +24,7 @@
     score_scale = head_dim ** (-0.5)
     running = jnp.full((head_count, 2, row_count), -1e30, jnp.float32)
     key_piece = lax.all_gather(keys, "ep", axis=0, tiled=True)
-    value_piece = lax.all_gather(values, "ep", axis=0, tiled=True)
+    value_piece = pass_along(values, "ep", 0)
     count = key_piece.shape[0]
     key_parts = key_piece.reshape(count, head_count, 2, head_dim)
     value_parts = value_piece.reshape(count, head_count, value_dim)

time: 184 us -> 171 us (0.929)
  blocking collectives: 67.5 us -> 40.3 us
  waiting for transfers between devices: 48 us -> 59.8 us
  local copies, waits for them, and re-layouts: 24.9 us -> 27.8 us
  starting transfers between devices: 4.81 us -> 6.84 us
    all_gather x1 -> x0, blocking collectives: 27.2 us -> none  [attend(): value_piece = lax.all_gather(values, 'ep', axis=0, tiled=True)]
    all_to_all x1, waiting for transfers between devices: 0.01 us -> 14.2 us  [experts(): back = lax.all_to_all(summed, 'ep', split_axis=1, concat_axis=1, tiled=True)]
    unnamed x3, waiting for transfers between devices: 20.3 us -> 8.66 us
    ppermute x0 -> x3, waiting for transfers between devices: none -> 9.29 us  [pass_along(): parts = [lax.ppermute(parts[0], name, right), *parts]]
    ppermute x0 -> x3, starting transfers between devices: none -> 2.18 us  [pass_along(): parts = [lax.ppermute(parts[0], name, right), *parts]]
    unnamed x26 -> x37, local copies, waits for them, and re-layouts: 10 us -> 11.3 us
  transfers between devices with their start and end apart: 3 -> 6, of which waited for: 2 -> 5; matrix products, arithmetic and copies ran while one was open for 5% -> 5% of each run, Pallas kernels for 0% -> 0%
where the time goes in v1:
time: 171 us
  waiting for transfers between devices  59.8 us (35%)
  blocking collectives  40.3 us (24%)
  local copies, waits for them, and re-layouts  27.8 us (16%)
  matrix products  16.1 us (9%)
  between operations  14.4 us (8%)
  starting transfers between devices  6.84 us (4%)
  other arithmetic  5.51 us (3%)
    all_gather x1, waiting for transfers between devices, experts(): piece = lax.all_gather(arrived, 'tp', axis=2, tiled=True)  27.7 us
    all_to_all x1, blocking collectives, experts(): lax.all_to_all(own_columns, 'ep', split_axis=0, concat_axis=0, tiled=True)  26.4 us
    all_to_all x1, waiting for transfers between devices, experts(): back = lax.all_to_all(summed, 'ep', split_axis=1, concat_axis=1, tiled=True)  14.2 us
    all_gather x1, blocking collectives, attend(): key_piece = lax.all_gather(keys, 'ep', axis=0, tiled=True)  13.9 us
    unnamed x37, local copies, waits for them, and re-layouts  11.3 us
    ppermute x3, waiting for transfers between devices, pass_along(): parts = [lax.ppermute(parts[0], name, right), *parts]  9.29 us
    unnamed x3, waiting for transfers between devices  8.66 us
    gather x1, local copies, waits for them, and re-layouts, experts(): outgoing = padded[owners].reshape(expert_count, capacity, width)  5.61 us
  transfers between devices with their start and end apart: 6, of which 5 were waited for; matrix products, arithmetic and copies ran while one was open for 5% of the time, Pallas kernels for 0%

profile of v1, /device:TPU:0, one launch (start us, length us, event | category | flops | bytes accessed | tf_op | source)
XLA Modules:
  0.0 170.7 jit_solution(6046883404924101542)
XLA Ops:
  7.2 0.0 copy-start
  7.2 0.0 all-gather.2.cloned.1.call-start
  7.2 1.0 copy.40
  8.2 0.1 eq.29
  8.3 0.1 reshape.111
  8.5 0.7 broadcast_multiply_fusion
  9.2 1.2 reduce-window.6
  10.4 0.2 slice_reduce_fusion
  10.6 0.2 reduce-window.9
  10.8 0.1 add_bitcast_fusion
  10.9 0.1 copy.44
  11.0 0.1 mul.105
  11.2 2.4 %scatter_custom_fusion = s32[1024]{0:T(1024)S(1)} fusion(s32[512]{0:T(512)S(1)} %bitcast.95, s32[512]{0:T(512)S(1)} %add_select_fusion, s32[]{:T(128)} %constant.90.clone.1), kind=kCustom, calls=%fused_computation.61 | custom fusion | bytes 4100 | tf_op jit(solution)/shard_map/scatter | solution.py:78
  13.7 1.4 fusion.8
  15.1 1.4 fusion.10
  16.4 0.1 concatenate.10
  16.5 5.6 %gather_fusion = bf16[1024,1536]{1,0:T(8,128)(2,1)} fusion(bf16[257,1536]{1,0:T(8,128)(2,1)S(1)} %concatenate.10, s32[1024]{0:T(1024)S(1)} %fusion.23), kind=kCustom, calls=%fused_computation | custom fusion | bytes 6295552 | tf_op jit(solution)/shard_map/gather | solution.py:81
  22.1 1.2 constant_dynamic-slice_fusion
  23.3 26.4 %all_to_all.17 = bf16[4,256,384]{2,1,0:T(8,128)(2,1)} all-to-all(bf16[4,256,384]{2,1,0:T(8,128)(2,1)S(1)} %constant_dynamic-slice_fusion), channel_id=1, replica_groups=mesh['grp'=2,'ep'=4,'tp'=4] {'ep'}, dimensions={0} | all-to-all | bytes 1572864 | tf_op jit(solution)/shard_map/all_to_all | solution.py:89
  49.7 0.0 all-gather.2.cloned.1.call-update
  49.7 0.0 reduce-scatter.4.cloned.1.call-start
  49.8 27.7 %all-gather.2.cloned.1.call-done = bf16[4,256,1536]{2,1,0:T(8,128)(2,1)} async-done(((bf16[4,256,384]{2,1,0:T(8,128)(2,1)}), bf16[4,256,1536]{2,1,0:T(8,128)(2,1)}) %all-gather.2.cloned.1.call-update) | async-done | bytes 3145744 | tf_op jit(solution)/shard_map/all_gather | solution.py:90
  77.5 5.4 %fusion.2 = f32[4,256,768]{2,1,0:T(8,128)S(1)} fusion(bf16[4,256,1536]{2,1,0:T(8,128)(2,1)} %all-gather.2.cloned.1.call-done, bf16[1,1536,768]{2,1,0:T(8,128)(2,1)} %param.22), kind=kOutput, calls=%fused_computation.7 | convolution fusion | flops 2415919104 | bytes 8650752 | tf_op jit(solution)/shard_map/scd,df->scf/dot_general | solution.py:92
  82.8 0.0 copy-done.10
  82.8 2.9 %multiply_convert_fusion = bf16[4,256,768]{2,1,0:T(8,128)(2,1)S(1)} fusion(f32[4,256,768]{2,1,0:T(8,128)S(1)} %fusion.2, bf16[4,256,1536]{2,1,0:T(8,128)(2,1)S(1)} %copy-done.10, bf16[1,1536,768]{2,1,0:T(8,128)(2,1)S(1)} %copy-done.11), kind=kOutput, calls=%fused_computation.5 | convolution fusion | flops 2420637696 | bytes 10223616 | tf_op jit(solution)/shard_map/scd,df->scf/dot_general | solution.py:91
  85.8 4.0 %fusion = bf16[1536,1024]{0,1:T(8,128)(2,1)} fusion(bf16[1024,768]{1,0:T(8,128)(2,1)S(1)} %bitcast.99, bf16[1,768,1536]{2,1,0:T(8,128)(2,1)S(1)} %copy-done), kind=kOutput, calls=%fused_computation.4 | convolution fusion | flops 2417491968 | bytes 7077888 | tf_op jit(solution)/shard_map/fd,sf->ds/dot_general | solution.py:96
  89.8 4.6 %copy.49 = bf16[1536,1024]{1,0:T(8,128)(2,1)} copy(bf16[1536,1024]{0,1:T(8,128)(2,1)} %fusion) | data formatting | bytes 6291456
  94.4 0.0 copy-start.7
  94.4 0.0 reduce-scatter.4.cloned.1.call-update
  94.5 0.8 copy-done.2
  95.3 1.5 collective-permute-start
  96.7 0.1 reduce_sum.43
  96.9 13.9 %all_gather.6 = bf16[512,256]{1,0:T(8,128)(2,1)S(1)} all-gather(bf16[128,256]{1,0:T(8,128)(2,1)S(1)} %copy-done.4), channel_id=1, replica_groups=mesh['grp'=2,'ep'=4,'tp'=4] {'ep'}, dimensions={0}, use_global_device_ids=true | all-gather | bytes 327680 | tf_op jit(solution)/shard_map/all_gather | solution.py:26
  110.8 0.1 copy.37
  110.9 0.1 copy.36
  111.1 0.1 copy.42
  111.2 0.4 fusion.30
  111.6 0.0 collective-permute-done
  111.6 0.7 collective-permute-start.1
  112.3 0.3 copy-done.1
  112.6 0.3 fusion.11
  112.9 0.8 copy.43
  113.7 0.8 copy.47
  114.5 3.2 %collective-permute-done.1 = bf16[128,256]{1,0:T(8,128)(2,1)S(1)} collective-permute-done((bf16[128,256]{1,0:T(8,128)(2,1)S(1)}, bf16[128,256]{1,0:T(8,128)(2,1)S(1)}, u32[]{:S(2)}, u32[]{:S(2)}) %collective-permute-start.1) | collective-permute-done | bytes 65568 | tf_op jit(solution)/shard_map/ppermute | solution.py:12
  117.7 0.0 collective-permute-start.2
  117.8 6.1 %collective-permute-done.2 = bf16[128,256]{1,0:T(8,128)(2,1)S(1)} collective-permute-done((bf16[128,256]{1,0:T(8,128)(2,1)S(1)}, bf16[128,256]{1,0:T(8,128)(2,1)S(1)}, u32[]{:S(2)}, u32[]{:S(2)}) %collective-permute-start.2) | collective-permute-done | bytes 65568 | tf_op jit(solution)/shard_map/ppermute | solution.py:12
  123.9 0.0 copy-start.8
  123.9 0.0 copy-start.9
  123.9 8.6 %reduce-scatter.4.cloned.1.call-done = bf16[384,1024]{1,0:T(8,128)(2,1)} async-done(((bf16[1536,1024]{1,0:T(8,128)(2,1)}), bf16[384,1024]{1,0:T(8,128)(2,1)}) %reduce-scatter.4.cloned.1.call-update) | async-done | bytes 786448
  132.5 2.3 %copy.50 = bf16[384,1024]{0,1:T(8,128)(2,1)} copy(bf16[384,1024]{1,0:T(8,128)(2,1)} %reduce-scatter.4.cloned.1.call-done) | data formatting | bytes 1572864
  134.8 4.6 %all-to-all-start.1 = ((bf16[384,4,256]{0,2,1:T(8,128)(2,1)}), bf16[384,4,256]{0,2,1:T(8,128)(2,1)S(1)}, u32[]{:S(2)}, u32[]{:S(2)}) async-start(bf16[384,4,256]{0,2,1:T(8,128)(2,1)} %bitcast.87), calls=%async_computation.1 | async-start | bytes 1572864 | tf_op jit(solution)/shard_map/all_to_all | solution.py:103
  139.4 0.6 constant_dynamic-update-slice_fusion.1
  140.0 0.6 constant_dynamic-update-slice_fusion
  140.6 1.0 constant_dynamic-slice_fusion.1
  141.6 0.9 copy.38
  142.5 1.7 %convolution_divide_fusion = f32[2,2,128,128]{2,3,1,0:T(8,128)S(1)} fusion(bf16[512,2,128,1]{0,2,3,1:T(8,128)(2,1)} %bitcast.91, f32[2,2,128,512]{3,2,1,0:T(8,128)} %copy-done.1, f32[2,2,128]{2,1,0:T(2,128)S(1)} %broadcast_maximum_fusion, f32[2,2,128]{2,1,0:T(2,128)S(1)} %fusion.11), kind=kOutput, calls=%fused_computation.17 | convolution fusion | flops 67698688 | bytes 1576960 | tf_op jit(solution)/shard_map/hcqk,khe->hcqe/dot_general | solution.py:38
  144.2 0.1 multiply_reduce_fusion
  144.3 0.1 multiply_convert_fusion.1
  144.4 0.7 copy.45
  145.2 14.2 %all-to-all-done.1 = bf16[384,4,256]{0,2,1:T(8,128)(2,1)S(1)} async-done(((bf16[384,4,256]{0,2,1:T(8,128)(2,1)}), bf16[384,4,256]{0,2,1:T(8,128)(2,1)S(1)}, u32[]{:S(2)}, u32[]{:S(2)}) %all-to-all-start.1) | async-done | bytes 786464 | tf_op jit(solution)/shard_map/all_to_all | solution.py:103
  159.3 1.9 %gather_fusion.1 = bf16[512,384]{1,0:T(8,128)(2,1)S(1)} fusion(bf16[384,1024]{0,1:T(8,128)(2,1)S(1)} %bitcast.85, s32[1024]{0:T(1024)S(1)} %pad_clamp_fusion), kind=kCustom, calls=%fused_computation.1 | custom fusion | bytes 788480 | tf_op jit(solution)/shard_map/jit(_take)/gather | solution.py:105
  161.3 0.1 gather.11
  161.4 1.7 %fusion.15 = bf16[256,1,384]{2,1,0:T(2,128)(2,1)S(1)} fusion(bf16[256,2,1]{1,2,0:T(2,128)(2,1)} %copy.47, bf16[384,256,2]{0,2,1:T(2,128)(2,1)S(1)} %gather.11, pred[256,2]{1,0:T(8,128)(4,1)} %copy.43), kind=kOutput, calls=%fused_computation.24 | convolution fusion | flops 589824 | bytes 591360 | tf_op jit(solution)/shard_map/drk,rk->rd/dot_general | solution.py:107
  163.2 0.7 copy.55
  (33 shorter events, 0.2 us)
Async XLA Ops:
  7.2 78.6 %copy-start = (bf16[1,768,1536]{2,1,0:T(8,128)(2,1)S(1)}, bf16[1,768,1536]{2,1,0:T(8,128)(2,1)}, u32[]{:S(2)}) copy-start(bf16[1,768,1536]{2,1,0:T(8,128)(2,1)} %param.23) | copy-start | bytes 7077892
  7.2 70.3 %all-gather.2.cloned.1.call-start = ((), (), s32[]{:S(2)}) async-start(), calls=%async_computation.3 | async-start | bytes 3932160 | tf_op jit(solution)/shard_map/all_gather | solution.py:90
  49.7 82.8 %reduce-scatter.4.cloned.1.call-start = ((), (), s32[]{:S(2)}) async-start(), calls=%async_computation.4 | async-start | bytes 3932160
  77.4 5.4 %copy-start.10 = (bf16[4,256,1536]{2,1,0:T(8,128)(2,1)S(1)}, bf16[4,256,1536]{2,1,0:T(8,128)(2,1)}, u32[]{:S(2)}) copy-start(bf16[4,256,1536]{2,1,0:T(8,128)(2,1)} %all-gather.2.cloned.1.call-done) | copy-start | bytes 9437188
  77.5 5.4 %copy-start.11 = (bf16[1,1536,768]{2,1,0:T(8,128)(2,1)S(1)}, bf16[1,1536,768]{2,1,0:T(8,128)(2,1)}, u32[]{:S(2)}) copy-start(bf16[1,1536,768]{2,1,0:T(8,128)(2,1)} %param.21) | copy-start | bytes 7077892
  94.4 0.8 copy-start.2
  94.4 2.5 %copy-start.4 = (bf16[128,256]{1,0:T(8,128)(2,1)S(1)}, bf16[128,256]{1,0:T(8,128)(2,1)}, u32[]{:S(2)}) copy-start(bf16[128,256]{1,0:T(8,128)(2,1)} %param.13) | copy-start | bytes 196612
  94.4 16.5 %copy-start.5 = (bf16[128,256]{1,0:T(8,128)(2,1)S(1)}, bf16[128,256]{1,0:T(8,128)(2,1)}, u32[]{:S(2)}) copy-start(bf16[128,256]{1,0:T(8,128)(2,1)} %param.12) | copy-start | bytes 196612
  94.4 16.7 %copy-start.6 = (s32[256,2]{0,1:T(2,128)S(1)}, s32[256,2]{0,1:T(2,128)}, u32[]{:S(2)}) copy-start(s32[256,2]{0,1:T(2,128)} %param.18) | copy-start | bytes 6148
  94.4 19.2 %copy-start.7 = (f32[256,2]{0,1:T(2,128)S(1)}, f32[256,2]{0,1:T(2,128)}, u32[]{:S(2)}) copy-start(f32[256,2]{0,1:T(2,128)} %param.19) | copy-start | bytes 6148
  95.3 16.4 %collective-permute-start = (bf16[128,256]{1,0:T(8,128)(2,1)S(1)}, bf16[128,256]{1,0:T(8,128)(2,1)S(1)}, u32[]{:S(2)}, u32[]{:S(2)}) collective-permute-start(bf16[128,256]{1,0:T(8,128)(2,1)S(1)} %copy-done.2), channel_id=1, source_target_pairs={{0,4},{4,8},{8,12},{12,0},{1,5},{5,9},{9,13},{13,1},{2,6},{6,10},{... | collective-permute-start | bytes 196616 | tf_op jit(solution)/shard_map/ppermute | solution.py:12
  111.6 1.0 copy-start.1
  111.6 6.1 %collective-permute-start.1 = (bf16[128,256]{1,0:T(8,128)(2,1)S(1)}, bf16[128,256]{1,0:T(8,128)(2,1)S(1)}, u32[]{:S(2)}, u32[]{:S(2)}) collective-permute-start(bf16[128,256]{1,0:T(8,128)(2,1)S(1)} %collective-permute-done), channel_id=1, source_target_pairs={{0,4},{4,8},{8,12},{12,0},{1,5},{5,9},{9,13},{13,1},{2,6},{6,10},{... | collective-permute-start | bytes 196616 | tf_op jit(solution)/shard_map/ppermute | solution.py:12
  117.7 6.1 %collective-permute-start.2 = (bf16[128,256]{1,0:T(8,128)(2,1)S(1)}, bf16[128,256]{1,0:T(8,128)(2,1)S(1)}, u32[]{:S(2)}, u32[]{:S(2)}) collective-permute-start(bf16[128,256]{1,0:T(8,128)(2,1)S(1)} %collective-permute-done.1), channel_id=1, source_target_pairs={{0,4},{4,8},{8,12},{12,0},{1,5},{5,9},{9,13},{13,1},{2,6},{6,10},{... | collective-permute-start | bytes 196616 | tf_op jit(solution)/shard_map/ppermute | solution.py:12
  123.9 10.9 %copy-start.3 = (bf16[1024,256]{1,0:T(8,128)(2,1)}, bf16[1024,256]{1,0:T(8,128)(2,1)S(1)}, u32[]{:S(2)}) copy-start(bf16[1024,256]{1,0:T(8,128)(2,1)S(1)} %constant_dynamic-update-slice_fusion.2) | copy-start | bytes 1572868
  123.9 20.3 %copy-start.8 = (f32[2]{0:T(128)S(1)}, f32[2]{0:T(128)}, u32[]{:S(2)}) copy-start(f32[2]{0:T(128)} %param.15) | copy-start | bytes 28
  123.9 20.4 %copy-start.9 = (f32[128]{0:T(128)S(1)}, f32[128]{0:T(128)}, u32[]{:S(2)}) copy-start(f32[128]{0:T(128)} %param.16) | copy-start | bytes 1540
  134.8 24.5 %all-to-all-start.1 = ((bf16[384,4,256]{0,2,1:T(8,128)(2,1)}), bf16[384,4,256]{0,2,1:T(8,128)(2,1)S(1)}, u32[]{:S(2)}, u32[]{:S(2)}) async-start(bf16[384,4,256]{0,2,1:T(8,128)(2,1)} %bitcast.87), calls=%async_computation.1 | async-start | bytes 1572864 | tf_op jit(solution)/shard_map/all_to_all | solution.py:103
Sparse Core Ops, SparseCore 0:
  49.8 27.5 all-gather.1
  94.6 37.9 reduce-scatter.3
